TPU v7x, 32 devices: a whole 2x2x4 slice. The times are simulated.
32 devices in a mesh: sp: 4 (over y, x), tp: 8 (over z, core).
Axes of the slice: x: 2, y: 2, z: 4, core: 2. Of those that a mesh axis runs over, the one named last changes fastest.
Arguments:
- target: bfloat16 [512, 2048], P('sp'), may hold values from -6 to 6
- source: bfloat16 [1536, 2048], P('sp'), may hold values from -6 to 6
- cotangent: bfloat16 [512, 2048], P('sp'), may hold values from -192 to 192
- target_gain: float32 [2048], replicated, may hold values from 0.1 to 1.9
- source_gain: float32 [2048], replicated, may hold values from 0.1 to 1.9
- w_query: bfloat16 [2048, 4096], P(None, 'tp'), may hold values from -0.125 to 0.125
- w_key: bfloat16 [2048, 128], replicated, may hold values from -0.125 to 0.125
- w_value: bfloat16 [2048, 128], replicated, may hold values from -0.125 to 0.125
- w_out: bfloat16 [4096, 2048], P('tp'), may hold values from -0.09375 to 0.09375
Outputs:
- grad_target: bfloat16 [512, 2048], P(('sp', 'tp'))
- grad_source: bfloat16 [1536, 2048], P(('sp', 'tp'))
- grad_out_w: bfloat16 [4096, 2048], P('tp', 'sp')
All inputs are finite; a program needn't handle non-finite values.
Results may differ from a plain program's by a relative error of at most 0.025.
Values may be sent and summed in bfloat16 or wider, within the bound.
A program may use at most 64 MiB of HBM per device.

v0:
```python
import jax
import jax.numpy as jnp
from jax import lax
from jax.sharding import PartitionSpec as P

HEAD = 128
NORM_EPS = 1e-06
KEY_BLOCK = 1024
QUERY_BLOCK = 256


def normed(row_block, gain_vec):
    rows_wide = row_block.astype(jnp.float32)
    inv_rms = lax.rsqrt(jnp.mean(rows_wide * rows_wide, axis=1, keepdims=True) + NORM_EPS)
    return (rows_wide * inv_rms * gain_vec).astype(jnp.bfloat16)


def norm_back(row_block, gain_vec, upstream):
    rows_wide = row_block.astype(jnp.float32)
    inv_rms = lax.rsqrt(jnp.mean(rows_wide * rows_wide, axis=1, keepdims=True) + NORM_EPS)
    unit_rows = rows_wide * inv_rms
    pulled = upstream * gain_vec
    return inv_rms * (pulled - unit_rows * jnp.mean(pulled * unit_rows, axis=1, keepdims=True))


def block_span(row_count, largest):
    if row_count > largest and row_count % largest == 0:
        return largest
    return row_count


def right_product(left_rows, weight_mat):
    return lax.dot_general(
        left_rows, weight_mat, (((1,), (1,)), ((), ())), preferred_element_type=jnp.float32
    )


def on_device(target, source, cotangent, target_gain, source_gain, w_query, w_key, w_value, w_out):
    tp_count = lax.axis_size("tp")
    tp_place = lax.axis_index("tp")
    group_rows = target.shape[0]
    q_width = w_query.shape[1]
    heads_here = q_width // HEAD
    inv_root = HEAD ** (-0.5)
    query_all = jnp.dot(
        normed(target, target_gain), w_query, preferred_element_type=jnp.float32
    ).astype(jnp.bfloat16)
    grad_all = right_product(cotangent, w_out).astype(jnp.bfloat16)
    cot_columns = lax.all_to_all(cotangent, "sp", split_axis=1, concat_axis=0, tiled=True)
    source_rows = source.shape[0] // tp_count
    source_part = lax.dynamic_slice_in_dim(source, tp_place * source_rows, source_rows, 0)
    source_normed = normed(source_part, source_gain)
    key_own = jnp.dot(source_normed, w_key, preferred_element_type=jnp.float32).astype(jnp.bfloat16)
    value_own = jnp.dot(source_normed, w_value, preferred_element_type=jnp.float32).astype(
        jnp.bfloat16
    )
    key_group, value_group = (
        lax.all_gather(key_own, "tp", axis=0, tiled=True),
        lax.all_gather(value_own, "tp", axis=0, tiled=True),
    )
    query_heads = query_all.reshape(group_rows, heads_here, HEAD)
    grad_heads = grad_all.reshape(group_rows, heads_here, HEAD)
    empty_stat = jnp.zeros((group_rows, heads_here), jnp.float32)
    empty_acc = jnp.zeros((group_rows, heads_here, HEAD), jnp.float32)
    start_state = (empty_stat, empty_acc, empty_acc, empty_acc)
    key_piece = lax.all_gather(key_group, "sp", axis=0, tiled=True)
    value_piece = lax.all_gather(value_group, "sp", axis=0, tiled=True)
    piece_rows = key_piece.shape[0]
    step_rows = block_span(piece_rows, KEY_BLOCK)

    def attend_one_block(block_index, loop_state):
        row_total, output_sum, tilted_sum, weight_sum = loop_state
        key_block = lax.dynamic_slice_in_dim(key_piece, block_index * step_rows, step_rows, 0)
        value_block = lax.dynamic_slice_in_dim(value_piece, block_index * step_rows, step_rows, 0)
        scores = (
            jnp.einsum("ihd,jd->ihj", query_heads, key_block, preferred_element_type=jnp.float32)
            * inv_root
        )
        exponent = jnp.exp(scores)
        weights = exponent.astype(jnp.bfloat16)
        prob_grad = jnp.einsum(
            "ihd,jd->ihj", grad_heads, value_block, preferred_element_type=jnp.float32
        )
        tilted = (exponent * prob_grad).astype(jnp.bfloat16)
        row_total = row_total + jnp.sum(exponent, axis=2)
        output_sum = output_sum + jnp.einsum(
            "ihj,jd->ihd", weights, value_block, preferred_element_type=jnp.float32
        )
        tilted_sum = tilted_sum + jnp.einsum(
            "ihj,jd->ihd", tilted, key_block, preferred_element_type=jnp.float32
        )
        weight_sum = weight_sum + jnp.einsum(
            "ihj,jd->ihd", weights, key_block, preferred_element_type=jnp.float32
        )
        return (row_total, output_sum, tilted_sum, weight_sum)

    row_total, output_sum, tilted_sum, weight_sum = lax.fori_loop(
        0, piece_rows // step_rows, attend_one_block, start_state
    )
    attended = (output_sum / row_total[:, :, None]).astype(jnp.bfloat16)
    delta_row = jnp.sum(attended.astype(jnp.float32) * grad_heads.astype(jnp.float32), axis=2)
    grad_query = (
        (tilted_sum - delta_row[:, :, None] * weight_sum) / row_total[:, :, None] * inv_root
    ).astype(jnp.bfloat16)
    all_total, all_delta = (
        lax.all_gather(row_total, "sp", axis=0, tiled=True),
        lax.all_gather(delta_row, "sp", axis=0, tiled=True),
    )
    empty_keys = jnp.zeros((key_group.shape[0], HEAD), jnp.float32)
    query_piece = lax.all_gather(query_all, "sp", axis=0, tiled=True)
    grad_piece = lax.all_gather(grad_all, "sp", axis=0, tiled=True)
    piece_rows = query_piece.shape[0]
    collect_step_rows = block_span(piece_rows, QUERY_BLOCK)

    def collect_one_block(block_index, loop_state):
        key_grad, value_grad = loop_state
        local_begin = block_index * collect_step_rows
        query_block = lax.dynamic_slice_in_dim(
            query_piece, local_begin, collect_step_rows, 0
        ).reshape(collect_step_rows, heads_here, HEAD)
        grad_block = lax.dynamic_slice_in_dim(
            grad_piece, local_begin, collect_step_rows, 0
        ).reshape(collect_step_rows, heads_here, HEAD)
        total_block = lax.dynamic_slice_in_dim(all_total, local_begin, collect_step_rows, 0)
        delta_block = lax.dynamic_slice_in_dim(all_delta, local_begin, collect_step_rows, 0)
        scores = (
            jnp.einsum("ihd,jd->ihj", query_block, key_group, preferred_element_type=jnp.float32)
            * inv_root
        )
        prob_rows = jnp.exp(scores) / total_block[:, :, None]
        prob_grad = jnp.einsum(
            "ihd,jd->ihj", grad_block, value_group, preferred_element_type=jnp.float32
        )
        score_grad = (prob_rows * (prob_grad - delta_block[:, :, None])).astype(jnp.bfloat16)
        key_grad = (
            key_grad
            + jnp.einsum("ihj,ihd->jd", score_grad, query_block, preferred_element_type=jnp.float32)
            * inv_root
        )
        value_grad = value_grad + jnp.einsum(
            "ihj,ihd->jd",
            prob_rows.astype(jnp.bfloat16),
            grad_block,
            preferred_element_type=jnp.float32,
        )
        return (key_grad, value_grad)

    key_grad, value_grad = lax.fori_loop(
        0, piece_rows // collect_step_rows, collect_one_block, (empty_keys, empty_keys)
    )
    key_sum, value_sum = (
        lax.psum_scatter(
            key_grad.astype(jnp.bfloat16), "tp", scatter_dimension=0, tiled=True
        ).astype(jnp.float32),
        lax.psum_scatter(
            value_grad.astype(jnp.bfloat16), "tp", scatter_dimension=0, tiled=True
        ).astype(jnp.float32),
    )
    pulled_source = right_product(key_sum.astype(jnp.bfloat16), w_key) + right_product(
        value_sum.astype(jnp.bfloat16), w_value
    )
    grad_source = norm_back(source_part, source_gain, pulled_source).astype(jnp.bfloat16)
    query_grad_rows = grad_query.reshape(group_rows, q_width)
    target_rows = group_rows // tp_count
    pulled_target = lax.psum_scatter(
        right_product(query_grad_rows, w_query).astype(jnp.bfloat16),
        "tp",
        scatter_dimension=0,
        tiled=True,
    ).astype(jnp.float32)
    target_part = lax.dynamic_slice_in_dim(target, tp_place * target_rows, target_rows, 0)
    grad_target = norm_back(target_part, target_gain, pulled_target).astype(jnp.bfloat16)
    attended_rows = attended.reshape(group_rows, q_width)
    grad_out = lax.dot_general(
        lax.all_gather(attended_rows, "sp", axis=0, tiled=True),
        cot_columns,
        (((0,), (0,)), ((), ())),
        preferred_element_type=jnp.float32,
    )
    return (grad_target, grad_source, grad_out.astype(jnp.bfloat16))


def solution(mesh):
    in_specs = (
        P("sp", None),
        P("sp", None),
        P("sp", None),
        P(),
        P(),
        P(None, "tp"),
        P(),
        P(),
        P("tp", None),
    )
    out_specs = (P(("sp", "tp"), None), P(("sp", "tp"), None), P("tp", "sp"))
    return jax.shard_map(
        on_device, mesh=mesh, in_specs=in_specs, out_specs=out_specs, check_vma=False
    )
```

profile of v0, /device:TPU:0, one launch (start us, length us, event | category | flops | bytes accessed | tf_op | source)
XLA Modules:
  0.0 221.8 jit_solution(9454115933237955824)
XLA Ops:
  7.2 0.0 copy-start
  7.2 0.0 reduce-scatter.6.cloned.1.call-start
  7.2 0.0 copy-start.8
  7.3 0.0 copy-start.12
  7.3 2.7 %convolution_convert_fusion.2 = bf16[128,512]{1,0:T(8,128)(2,1)S(1)} fusion(bf16[128,2048]{1,0:T(8,128)(2,1)} %param.13, bf16[512,2048]{1,0:T(8,128)(2,1)} %param.19), kind=kOutput, calls=%fused_computation.33 | convolution fusion | flops 268500992 | bytes 2752512 | tf_op jit(solution)/shard_map/dot_general | solution.py:33
  10.0 0.0 copy-start.13
  10.0 0.1 copy.61
  10.1 12.3 %all_gather.33 = bf16[512,512]{1,0:T(8,128)(2,1)} all-gather(bf16[128,512]{1,0:T(8,128)(2,1)S(1)} %convolution_convert_fusion.2), channel_id=1, replica_groups=mesh['sp'=4,'tp'=8] {'sp'}, dimensions={0}, use_global_device_ids=true | all-gather | bytes 655360 | tf_op jit(solution)/shard_map/all_gather | solution.py:111
  22.4 1.1 fusion.35
  23.6 1.2 convolution_convert_fusion.5
  24.8 14.1 %all_gather.27 = bf16[384,128]{1,0:T(8,128)(2,1)S(1)} all-gather(bf16[48,128]{1,0:T(8,128)(2,1)S(1)} %convolution_convert_fusion.5), channel_id=1, replica_groups=mesh['sp'=4,'tp'=8] {'tp'}, dimensions={0}, use_global_device_ids=true | all-gather | bytes 110592 | tf_op jit(solution)/shard_map/all_gather | solution.py:58
  38.9 9.4 %all_gather.28 = bf16[1536,128]{1,0:T(8,128)(2,1)S(1)} all-gather(bf16[384,128]{1,0:T(8,128)(2,1)S(1)} %all_gather.27), channel_id=1, replica_groups=mesh['sp'=4,'tp'=8] {'sp'}, dimensions={0}, use_global_device_ids=true | all-gather | bytes 491520 | tf_op jit(solution)/shard_map/all_gather | solution.py:66
  48.3 0.2 fusion.19
  48.5 0.5 convolution_convert_fusion.3
  49.0 10.1 %all_gather.31 = bf16[512,512]{1,0:T(8,128)(2,1)} all-gather(bf16[128,512]{1,0:T(8,128)(2,1)S(1)} %convolution_convert_fusion.3), channel_id=1, replica_groups=mesh['sp'=4,'tp'=8] {'sp'}, dimensions={0}, use_global_device_ids=true | all-gather | bytes 655360 | tf_op jit(solution)/shard_map/all_gather | solution.py:110
  59.1 0.0 copy-start.6
  59.2 0.7 fusion.55
  59.8 0.3 copy-done.6
  60.2 1.4 convolution_convert_fusion.4
  61.6 13.9 %all_gather.29 = bf16[384,128]{1,0:T(8,128)(2,1)S(1)} all-gather(bf16[48,128]{1,0:T(8,128)(2,1)S(1)} %convolution_convert_fusion.4), channel_id=1, replica_groups=mesh['sp'=4,'tp'=8] {'tp'}, dimensions={0}, use_global_device_ids=true | all-gather | bytes 110592 | tf_op jit(solution)/shard_map/all_gather | solution.py:59
  75.5 9.8 %all_gather.30 = bf16[1536,128]{1,0:T(8,128)(2,1)S(1)} all-gather(bf16[384,128]{1,0:T(8,128)(2,1)S(1)} %all_gather.29), channel_id=1, replica_groups=mesh['sp'=4,'tp'=8] {'sp'}, dimensions={0}, use_global_device_ids=true | all-gather | bytes 491520 | tf_op jit(solution)/shard_map/all_gather | solution.py:67
  85.3 6.8 %all_gather.32 = f32[512,4]{0,1:T(4,128)S(1)} all-gather(f32[128,4]{0,1:T(4,128)S(1)} %get-tuple-element.260), channel_id=1, replica_groups=mesh['sp'=4,'tp'=8] {'sp'}, dimensions={0}, use_global_device_ids=true | all-gather | bytes 10240 | tf_op jit(solution)/shard_map/all_gather | solution.py:106
  92.1 1.3 multiply_reduce_fusion
  93.4 8.4 %all_gather.34 = f32[512,4]{0,1:T(4,128)S(1)} all-gather(f32[128,4]{0,1:T(4,128)S(1)} %get-tuple-element.262), channel_id=1, replica_groups=mesh['sp'=4,'tp'=8] {'sp'}, dimensions={0}, use_global_device_ids=true | all-gather | bytes 10240 | tf_op jit(solution)/shard_map/all_gather | solution.py:107
  101.8 16.5 %while.10 = (s32[]{:T(128)}, f32[384,128]{1,0:T(8,128)S(1)}, f32[384,128]{1,0:T(8,128)S(1)}, bf16[512,512]{1,0:T(8,128)(2,1)}, bf16[384,128]{1,0:T(8,128)(2,1)},...) while((s32[]{:T(128)}, f32[384,128]{1,0:T(8,128)S(1)}, ...), condition=%wide.region_8.0_spmd.clone, body=%wide.region_7.0_spmd.clone.sunk | while | flops 405258240 | bytes 8872134 | solution.py:148
  101.8 1.1 constant_dynamic-slice_fusion.6
  102.9 0.1 copy.71
  103.0 2.5 %exponential_divide_fusion.2 = f32[256,4,384]{2,0,1:T(8,128)} fusion(bf16[256,4,128]{0,2,1:T(8,128)(2,1)S(1)} %bitcast.95, f32[256,4]{0,1:T(4,128)S(1)} %get-tuple-element.326, bf16[384,128]{1,0:T(8,128)(2,1)} %get-tuple-element.359), kind=kOutput, calls=%fused_computation.1.clone.1 | convolution fusion | flops 101449728 | bytes 1937408 | tf_op jit(solution)/shard_map/while/body/eval_jaxpr/ihd,jd->ihj/dot_general | solution.py:127
  105.6 0.1 copy.72
  105.7 2.5 %fusion.92 = f32[384,128]{1,0:T(8,128)S(1)} fusion(bf16[256,4,128]{0,2,1:T(8,128)(2,1)S(1)} %bitcast.96, f32[256,4,384]{2,0,1:T(8,128)} %exponential_divide_fusion.2, bf16[256,4,128]{0,2,1:T(8,128)(2,1)S(1)} %bitcast.93, f32[256,4]{0,1:T(4,128)S(1)} %get-tuple-element.328, f32[384,128]{1,0:T(8,128)S(1)} %get-tuple-element.343, ...), kind=kOutput, calls=%fused_computation.6.clone.1 | convolution fusion | flops 202653696 | bytes 2592769 | tf_op jit(solution)/shard_map/while/body/eval_jaxpr/ihj,ihd->jd/dot_general | solution.py:137
  108.2 1.8 fusion.93
  110.1 1.1 constant_dynamic-slice_fusion.6
  111.1 0.1 copy.71
  111.3 2.6 %exponential_divide_fusion.2 = f32[256,4,384]{2,0,1:T(8,128)} fusion(bf16[256,4,128]{0,2,1:T(8,128)(2,1)S(1)} %bitcast.95, f32[256,4]{0,1:T(4,128)S(1)} %get-tuple-element.326, bf16[384,128]{1,0:T(8,128)(2,1)} %get-tuple-element.359), kind=kOutput, calls=%fused_computation.1.clone.1 | convolution fusion | flops 101449728 | bytes 1937408 | tf_op jit(solution)/shard_map/while/body/eval_jaxpr/ihd,jd->ihj/dot_general | solution.py:127
  113.9 0.1 copy.72
  114.0 2.5 %fusion.92 = f32[384,128]{1,0:T(8,128)S(1)} fusion(bf16[256,4,128]{0,2,1:T(8,128)(2,1)S(1)} %bitcast.96, f32[256,4,384]{2,0,1:T(8,128)} %exponential_divide_fusion.2, bf16[256,4,128]{0,2,1:T(8,128)(2,1)S(1)} %bitcast.93, f32[256,4]{0,1:T(4,128)S(1)} %get-tuple-element.328, f32[384,128]{1,0:T(8,128)S(1)} %get-tuple-element.343, ...), kind=kOutput, calls=%fused_computation.6.clone.1 | convolution fusion | flops 202653696 | bytes 2592769 | tf_op jit(solution)/shard_map/while/body/eval_jaxpr/ihj,ihd->jd/dot_general | solution.py:137
  116.5 1.8 fusion.93
  118.3 0.6 convert_element_type.105
  119.0 0.0 reduce-scatter.6.cloned.1.call-update
  119.0 2.0 copy.45
  121.1 4.1 %all-to-all-start = ((bf16[128,4,512]{0,2,1:T(8,128)(2,1)}), bf16[128,4,512]{0,2,1:T(8,128)(2,1)}, u32[]{:S(2)}, u32[]{:S(2)}) async-start(bf16[128,4,512]{0,2,1:T(8,128)(2,1)} %bitcast.7), calls=%async_computation.3 | async-start | bytes 1048576 | tf_op jit(solution)/shard_map/all_to_all | solution.py:49
  125.2 0.0 reduce-scatter.8.cloned.1.call-start
  125.2 0.6 convert_element_type.106
  125.9 0.1 reduce-scatter.8.cloned.1.call-update
  126.0 0.0 reduce-scatter.4.cloned.1.call-start
  126.0 2.6 %convolution_multiply_fusion.2 = f32[128,4,128]{0,2,1:T(8,128)S(1)} fusion(f32[128,4,1536]{2,0,1:T(8,128)} %copy-done.1, bf16[1536,128]{1,0:T(8,128)(2,1)S(1)} %copy-done.3, f32[128,4]{0,1:T(4,128)S(1)} %get-tuple-element.262), kind=kOutput, calls=%fused_computation.28 | convolution fusion | flops 202178560 | bytes 3803136 | tf_op jit(solution)/shard_map/while/body/eval_jaxpr/ihj,jd->ihd/dot_general | solution.py:92
  128.6 3.6 %fusion.17 = bf16[128,4,128]{0,2,1:T(8,128)(2,1)} fusion(f32[128,4,128]{0,2,1:T(8,128)S(1)} %convolution_multiply_fusion.2, f32[128,4,1536]{2,0,1:T(8,128)} %copy-done.1, bf16[128,4,128]{0,2,1:T(8,128)(2,1)S(1)} %bitcast.98, bf16[1536,128]{1,0:T(8,128)(2,1)S(1)} %copy-done.5, bf16[1536,128]{1,0:T(8,128)(2,1)S(1)} %copy-done.3, ...), kind=kOutput, calls=%fused_computation.32 | convolution fusion | flops 404488192 | bytes 4458496 | tf_op jit(solution)/shard_map/while/body/eval_jaxpr/ihj,jd->ihd/dot_general | solution.py:89
  132.2 2.6 %convolution_convert_fusion = bf16[128,2048]{1,0:T(8,128)(2,1)} fusion(bf16[128,512]{0,1:T(8,128)(2,1)} %bitcast.100, bf16[2048,512]{1,0:T(8,128)(2,1)S(1)} %copy-done), kind=kOutput, calls=%fused_computation.20 | convolution fusion | flops 268697600 | bytes 2752512 | tf_op jit(solution)/shard_map/dot_general | solution.py:33
  134.8 0.0 reduce-scatter.4.cloned.1.call-update
  134.8 1.0 fusion.48
  135.8 0.5 add_rsqrt_fusion.2
  136.4 10.5 %all_gather.35 = bf16[512,512]{0,1:T(8,128)(2,1)S(1)} all-gather(bf16[128,512]{0,1:T(8,128)(2,1)S(1)} %bitcast.99), channel_id=1, replica_groups=mesh['sp'=4,'tp'=8] {'sp'}, dimensions={0}, use_global_device_ids=true | all-gather | bytes 655360 | tf_op jit(solution)/shard_map/all_gather | solution.py:175
  146.9 2.9 %reduce-scatter.6.cloned.1.call-done = bf16[48,128]{1,0:T(8,128)(2,1)} async-done(((bf16[384,128]{1,0:T(8,128)(2,1)}), bf16[48,128]{1,0:T(8,128)(2,1)}) %reduce-scatter.6.cloned.1.call-update) | async-done | bytes 12304 | tf_op jit(solution)/shard_map/reduce_scatter | solution.py:152
  149.8 1.3 fusion.56
  151.1 29.6 %reduce-scatter.8.cloned.1.call-done = bf16[48,128]{1,0:T(8,128)(2,1)} async-done(((bf16[384,128]{1,0:T(8,128)(2,1)}), bf16[48,128]{1,0:T(8,128)(2,1)}) %reduce-scatter.8.cloned.1.call-update) | async-done | bytes 12304 | tf_op jit(solution)/shard_map/reduce_scatter | solution.py:155
  180.7 1.3 fusion.31
  182.1 0.0 copy-start.15
  182.1 1.8 fusion.34
  183.9 0.0 all-to-all-done
  183.9 1.2 copy.46
  185.1 1.2 convolution_convert_fusion.1
  186.4 26.2 %reduce-scatter.4.cloned.1.call-done = bf16[16,2048]{1,0:T(8,128)(2,1)} async-done(((bf16[128,2048]{1,0:T(8,128)(2,1)}), bf16[16,2048]{1,0:T(8,128)(2,1)}) %reduce-scatter.4.cloned.1.call-update) | async-done | bytes 65552 | tf_op jit(solution)/shard_map/reduce_scatter | solution.py:165
  212.6 1.1 fusion.44
  213.7 1.6 fusion.47
  (33 shorter events, 0.1 us)
Async XLA Ops:
  7.2 41.4 %copy-start = (bf16[2048,512]{1,0:T(8,128)(2,1)S(1)}, bf16[2048,512]{1,0:T(8,128)(2,1)}, u32[]{:S(2)}) copy-start(bf16[2048,512]{1,0:T(8,128)(2,1)} %param.16) | copy-start | bytes 6291460
  7.2 142.6 %reduce-scatter.6.cloned.1.call-start = ((), (), s32[]{:S(2)}) async-start(), calls=%async_computation.5 | async-start | bytes 110592 | tf_op jit(solution)/shard_map/reduce_scatter | solution.py:152
  7.2 16.3 %copy-start.8 = (bf16[2048,128]{1,0:T(8,128)(2,1)S(1)}, bf16[2048,128]{1,0:T(8,128)(2,1)}, u32[]{:S(2)}) copy-start(bf16[2048,128]{1,0:T(8,128)(2,1)} %param.17) | copy-start | bytes 1572868
  7.3 16.3 %copy-start.12 = (f32[2048]{0:T(1024)S(1)}, f32[2048]{0:T(1024)}, u32[]{:S(2)}) copy-start(f32[2048]{0:T(1024)} %param.15) | copy-start | bytes 24580
  10.0 38.5 %copy-start.13 = (f32[2048]{0:T(1024)S(1)}, f32[2048]{0:T(1024)}, u32[]{:S(2)}) copy-start(f32[2048]{0:T(1024)} %param.14) | copy-start | bytes 24580
  22.4 25.9 %copy-start.9 = (bf16[128,2048]{1,0:T(8,128)(2,1)S(1)}, bf16[128,2048]{1,0:T(8,128)(2,1)}, u32[]{:S(2)}) copy-start(bf16[128,2048]{1,0:T(8,128)(2,1)} %param.11) | copy-start | bytes 1572868
  23.6 36.3 %copy-start.14 = (f32[48]{0:T(128)}, f32[48]{0:T(128)S(1)}, u32[]{:S(2)}) copy-start(f32[48]{0:T(128)S(1)} %add_rsqrt_fusion) | copy-start | bytes 580
  38.9 9.6 %copy-start.11 = (bf16[384,128]{1,0:T(8,128)(2,1)}, bf16[384,128]{1,0:T(8,128)(2,1)S(1)}, u32[]{:S(2)}) copy-start(bf16[384,128]{1,0:T(8,128)(2,1)S(1)} %all_gather.27) | copy-start | bytes 294916
  48.3 10.8 %copy-start.2 = (bf16[1536,128]{1,0:T(8,128)(2,1)}, bf16[1536,128]{1,0:T(8,128)(2,1)S(1)}, u32[]{:S(2)}) copy-start(bf16[1536,128]{1,0:T(8,128)(2,1)S(1)} %all_gather.28) | copy-start | bytes 1179652
  59.1 1.0 copy-start.6
  60.2 33.3 %copy-start.1 = (f32[128,4,1536]{2,0,1:T(8,128)}, f32[128,4,1536]{2,0,1:T(8,128)S(1)}, u32[]{:S(2)}) copy-start(f32[128,4,1536]{2,0,1:T(8,128)S(1)} %get-tuple-element.261) | copy-start | bytes 9437188
  85.3 8.1 %copy-start.4 = (bf16[1536,128]{1,0:T(8,128)(2,1)}, bf16[1536,128]{1,0:T(8,128)(2,1)S(1)}, u32[]{:S(2)}) copy-start(bf16[1536,128]{1,0:T(8,128)(2,1)S(1)} %all_gather.30) | copy-start | bytes 1179652
  118.3 7.7 %copy-start.3 = (bf16[1536,128]{1,0:T(8,128)(2,1)S(1)}, bf16[1536,128]{1,0:T(8,128)(2,1)}, u32[]{:S(2)}) copy-start(bf16[1536,128]{1,0:T(8,128)(2,1)} %copy-done.2) | copy-start | bytes 1179652
  121.1 62.8 %all-to-all-start = ((bf16[128,4,512]{0,2,1:T(8,128)(2,1)}), bf16[128,4,512]{0,2,1:T(8,128)(2,1)}, u32[]{:S(2)}, u32[]{:S(2)}) async-start(bf16[128,4,512]{0,2,1:T(8,128)(2,1)} %bitcast.7), calls=%async_computation.3 | async-start | bytes 1048576 | tf_op jit(solution)/shard_map/all_to_all | solution.py:49
  125.2 55.6 %reduce-scatter.8.cloned.1.call-start = ((), (), s32[]{:S(2)}) async-start(), calls=%async_computation.6 | async-start | bytes 110592 | tf_op jit(solution)/shard_map/reduce_scatter | solution.py:155
  125.9 2.7 %copy-start.5 = (bf16[1536,128]{1,0:T(8,128)(2,1)S(1)}, bf16[1536,128]{1,0:T(8,128)(2,1)}, u32[]{:S(2)}) copy-start(bf16[1536,128]{1,0:T(8,128)(2,1)} %copy-done.4) | copy-start | bytes 1179652
  126.0 86.7 %reduce-scatter.4.cloned.1.call-start = ((), (), s32[]{:S(2)}) async-start(), calls=%async_computation.4 | async-start | bytes 589824 | tf_op jit(solution)/shard_map/reduce_scatter | solution.py:165
  132.2 4.1 %copy-start.10 = (bf16[128,4,128]{0,2,1:T(8,128)(2,1)S(1)}, bf16[128,4,128]{0,2,1:T(8,128)(2,1)}, u32[]{:S(2)}) copy-start(bf16[128,4,128]{0,2,1:T(8,128)(2,1)} %get-tuple-element.263) | copy-start | bytes 393220
  134.8 46.0 %copy-start.7 = (bf16[2048,128]{1,0:T(8,128)(2,1)S(1)}, bf16[2048,128]{1,0:T(8,128)(2,1)}, u32[]{:S(2)}) copy-start(bf16[2048,128]{1,0:T(8,128)(2,1)} %param.18) | copy-start | bytes 1572868
  182.1 30.5 %copy-start.15 = (f32[16]{0:T(128)S(1)}, f32[16]{0:T(128)}, u32[]{:S(2)}) copy-start(f32[16]{0:T(128)} %add_rsqrt_fusion.2) | copy-start | bytes 196
Sparse Core Ops, SparseCore 0:
  119.1 30.5 reduce-scatter.5
  152.0 28.7 reduce-scatter.7
  183.0 29.5 reduce-scatter.3
where the time goes:
time: 223 us; the launch traced here: 222 us
  blocking collectives  95.2 us (43%)
  waiting for transfers between devices  58.9 us (26%)
  matrix products  34.2 us (15%)
  between operations  14 us (6%)
  other arithmetic  8.6 us (4%)
  local copies, waits for them, and re-layouts  6.51 us (3%)
  starting transfers between devices  4.25 us (2%)
    reduce_scatter x1, waiting for transfers between devices, on_device(): lax.psum_scatter(value_grad.astype(jnp.bfloat16), 'tp', scatter_dimension...  29.6 us
    reduce_scatter x1, waiting for transfers between devices, on_device(): lax.psum_scatter(right_product(query_grad_rows, w_query).astype(jnp.bfloa...  26.2 us
    all_gather x1, blocking collectives, on_device(): lax.all_gather(key_own, 'tp', axis=0, tiled=True)  14.1 us
    all_gather x1, blocking collectives, on_device(): lax.all_gather(value_own, 'tp', axis=0, tiled=True)  13.9 us
    all_gather x1, blocking collectives, on_device(): grad_piece = lax.all_gather(grad_all, 'sp', axis=0, tiled=True)  12.3 us
    all_gather x1, blocking collectives, on_device(): lax.all_gather(attended_rows, 'sp', axis=0, tiled=True)  10.5 us
    all_gather x1, blocking collectives, on_device(): query_piece = lax.all_gather(query_all, 'sp', axis=0, tiled=True)  10.1 us
    all_gather x1, blocking collectives, on_device(): value_piece = lax.all_gather(value_group, 'sp', axis=0, tiled=True)  9.79 us
  transfers between devices with their start and end apart: 4, of which 3 were waited for; matrix products, arithmetic and copies ran while one was open for 9% of the time, Pallas kernels for 0%

commit v1 on v0

--- a/solution.py
+++ b/solution.py
@@ -108,7 +108,12 @@
     )
     empty_keys = jnp.zeros((key_group.shape[0], HEAD), jnp.float32)
     query_piece = lax.all_gather(query_all, "sp", axis=0, tiled=True)
-    grad_piece = lax.all_gather(grad_all, "sp", axis=0, tiled=True)
+    ring = [grad_all]
+    for hop in range(3):
+        ring.append(lax.ppermute(ring[-1], "sp", [(dev, (dev + 1) % 4) for dev in range(4)]))
+    grad_piece = jnp.roll(
+        jnp.concatenate(ring[::-1], axis=0), (lax.axis_index("sp") + 1) * ring[0].shape[0], axis=0
+    )
     piece_rows = query_piece.shape[0]
     collect_step_rows = block_span(piece_rows, QUERY_BLOCK)
 

time: 223 us -> 230 us (1.031)
  blocking collectives: 95.2 us -> 83.8 us
  waiting for transfers between devices: 58.9 us -> 70.2 us
  starting transfers between devices: 4.25 us -> 8.03 us
    all_gather x1 -> x0, blocking collectives: 12.3 us -> none  [on_device(): grad_piece = lax.all_gather(grad_all, 'sp', axis=0, tiled=True)]
    reduce_scatter x1, waiting for transfers between devices: 2.91 us -> 9.84 us  [on_device(): lax.psum_scatter(key_grad.astype(jnp.bfloat16), 'tp', scatter_dimension=0...]
    ppermute x0 -> x3, starting transfers between devices: none -> 3.64 us  [on_device(): lax.ppermute(ring[-1], 'sp', [(dev, (dev + 1) % 4) for dev in range(4)])]
  transfers between devices with their start and end apart: 4 -> 7, of which waited for: 3 -> 4; matrix products, arithmetic and copies ran while one was open for 9% -> 21% of each run, Pallas kernels for 0% -> 0%
where the time goes in v1:
time: 230 us; the launch traced here: 229 us
  blocking collectives  83.8 us (36%)
  waiting for transfers between devices  70.2 us (31%)
  matrix products  36.1 us (16%)
  between operations  14.1 us (6%)
  local copies, waits for them, and re-layouts  8.73 us (4%)
  starting transfers between devices  8.03 us (3%)
  other arithmetic  7.97 us (3%)
    reduce_scatter x1, waiting for transfers between devices, on_device(): lax.psum_scatter(value_grad.astype(jnp.bfloat16), 'tp', scatter_dimension...  29.7 us
    reduce_scatter x1, waiting for transfers between devices, on_device(): lax.psum_scatter(right_product(query_grad_rows, w_query).astype(jnp.bfloa...  28.5 us
    all_gather x1, blocking collectives, on_device(): lax.all_gather(key_own, 'tp', axis=0, tiled=True)  14.2 us
    all_gather x1, blocking collectives, on_device(): lax.all_gather(value_own, 'tp', axis=0, tiled=True)  13.9 us
    all_gather x1, blocking collectives, on_device(): lax.all_gather(attended_rows, 'sp', axis=0, tiled=True)  9.93 us
    all_gather x1, blocking collectives, on_device(): key_piece = lax.all_gather(key_group, 'sp', axis=0, tiled=True)  9.91 us
    reduce_scatter x1, waiting for transfers between devices, on_device(): lax.psum_scatter(key_grad.astype(jnp.bfloat16), 'tp', scatter_dimension=0...  9.84 us
    all_gather x1, blocking collectives, on_device(): query_piece = lax.all_gather(query_all, 'sp', axis=0, tiled=True)  9.79 us
  transfers between devices with their start and end apart: 7, of which 4 were waited for; matrix products, arithmetic and copies ran while one was open for 21% of the time, Pallas kernels for 0%

profile of v1, /device:TPU:0, one launch (start us, length us, event | category | flops | bytes accessed | tf_op | source)
XLA Modules:
  0.0 229.0 jit_solution(1760139788541956099)
XLA Ops:
  7.2 0.0 copy-start
  7.2 2.7 %convolution_convert_fusion.2 = bf16[128,512]{1,0:T(8,128)(2,1)S(1)} fusion(bf16[128,2048]{1,0:T(8,128)(2,1)} %param.13, bf16[512,2048]{1,0:T(8,128)(2,1)} %param.19), kind=kOutput, calls=%fused_computation.33 | convolution fusion | flops 268500992 | bytes 2752512 | tf_op jit(solution)/shard_map/dot_general | solution.py:33
  9.9 0.0 copy-start.13
  10.0 3.0 %collective-permute-start = (bf16[128,512]{1,0:T(8,128)(2,1)S(1)}, bf16[128,512]{1,0:T(8,128)(2,1)}, u32[]{:S(2)}, u32[]{:S(2)}) collective-permute-start(bf16[128,512]{1,0:T(8,128)(2,1)S(1)} %convolution_convert_fusion.2), channel_id=1, source_target_pairs={{0,8},{8,16},{16,24},{24,0},{1,9},{9,17},{17,25},{25,1},{2,10},{10... | collective-permute-start | bytes 393224 | tf_op jit(solution)/shard_map/ppermute | solution.py:113
  13.0 1.0 copy.45
  14.0 4.3 %all-to-all-start = ((bf16[128,4,512]{0,2,1:T(8,128)(2,1)}), bf16[128,4,512]{0,2,1:T(8,128)(2,1)}, u32[]{:S(2)}, u32[]{:S(2)}) async-start(bf16[128,4,512]{0,2,1:T(8,128)(2,1)} %bitcast.7), calls=%async_computation.3 | async-start | bytes 1048576 | tf_op jit(solution)/shard_map/all_to_all | solution.py:49
  18.3 0.0 reduce-scatter.6.cloned.1.call-start
  18.3 1.1 fusion.35
  19.4 1.2 convolution_convert_fusion.5
  20.6 14.2 %all_gather.24 = bf16[384,128]{1,0:T(8,128)(2,1)S(1)} all-gather(bf16[48,128]{1,0:T(8,128)(2,1)S(1)} %convolution_convert_fusion.5), channel_id=1, replica_groups=mesh['sp'=4,'tp'=8] {'tp'}, dimensions={0}, use_global_device_ids=true | all-gather | bytes 110592 | tf_op jit(solution)/shard_map/all_gather | solution.py:58
  34.8 9.9 %all_gather.25 = bf16[1536,128]{1,0:T(8,128)(2,1)S(1)} all-gather(bf16[384,128]{1,0:T(8,128)(2,1)S(1)} %all_gather.24), channel_id=1, replica_groups=mesh['sp'=4,'tp'=8] {'sp'}, dimensions={0}, use_global_device_ids=true | all-gather | bytes 491520 | tf_op jit(solution)/shard_map/all_gather | solution.py:66
  44.7 0.2 fusion.19
  44.9 0.5 convolution_convert_fusion.3
  45.4 0.0 copy-start.10
  45.5 2.3 fusion.55
  47.7 1.2 convolution_convert_fusion.4
  48.9 0.1 copy.61
  49.1 13.9 %all_gather.26 = bf16[384,128]{1,0:T(8,128)(2,1)S(1)} all-gather(bf16[48,128]{1,0:T(8,128)(2,1)S(1)} %convolution_convert_fusion.4), channel_id=1, replica_groups=mesh['sp'=4,'tp'=8] {'tp'}, dimensions={0}, use_global_device_ids=true | all-gather | bytes 110592 | tf_op jit(solution)/shard_map/all_gather | solution.py:59
  63.0 9.4 %all_gather.27 = bf16[1536,128]{1,0:T(8,128)(2,1)S(1)} all-gather(bf16[384,128]{1,0:T(8,128)(2,1)S(1)} %all_gather.26), channel_id=1, replica_groups=mesh['sp'=4,'tp'=8] {'sp'}, dimensions={0}, use_global_device_ids=true | all-gather | bytes 491520 | tf_op jit(solution)/shard_map/all_gather | solution.py:67
  72.5 0.6 collective-permute-start.1
  73.1 3.4 %multiply_reduce_fusion = (f32[128,4]{0,1:T(4,128)S(1)}, bf16[128,4,128]{0,2,1:T(8,128)(2,1)}) fusion(bf16[128,512]{0,1:T(8,128)(2,1)S(1)} %copy.61, f32[128,4]{0,1:T(4,128)S(1)} %get-tuple-element.260, bf16[1536,128]{1,0:T(8,128)(2,1)S(1)} %all_gather.27, f32[128,4,1536]{2,0,1:T(8,128)} %get-tuple-element.261), kind=kOutput, calls=%fused_computation.61 | convolution fusion | flops 202505728 | bytes 3805184 | tf_op jit(solution)/shard_map/while/body/eval_jaxpr/ihj,jd->ihd/dot_general | solution.py:86
  76.4 2.1 collective-permute-done.1
  78.6 0.0 copy-start.11
  78.6 1.4 convolution_multiply_fusion.2
  80.0 8.6 %all_gather.29 = f32[512,4]{0,1:T(4,128)S(1)} all-gather(f32[128,4]{0,1:T(4,128)S(1)} %get-tuple-element.260), channel_id=1, replica_groups=mesh['sp'=4,'tp'=8] {'sp'}, dimensions={0}, use_global_device_ids=true | all-gather | bytes 10240 | tf_op jit(solution)/shard_map/all_gather | solution.py:106
  88.6 8.1 %all_gather.30 = f32[512,4]{0,1:T(4,128)S(1)} all-gather(f32[128,4]{0,1:T(4,128)S(1)} %get-tuple-element.262), channel_id=1, replica_groups=mesh['sp'=4,'tp'=8] {'sp'}, dimensions={0}, use_global_device_ids=true | all-gather | bytes 10240 | tf_op jit(solution)/shard_map/all_gather | solution.py:107
  96.6 9.8 %all_gather.28 = bf16[512,512]{1,0:T(8,128)(2,1)} all-gather(bf16[128,512]{1,0:T(8,128)(2,1)S(1)} %copy-done.11), channel_id=1, replica_groups=mesh['sp'=4,'tp'=8] {'sp'}, dimensions={0}, use_global_device_ids=true | all-gather | bytes 655360 | tf_op jit(solution)/shard_map/all_gather | solution.py:110
  106.5 0.9 constant_dynamic-update-slice_fusion.5
  107.4 0.9 constant_dynamic-update-slice_fusion.1
  108.4 0.8 constant_dynamic-slice_fusion.4
  109.2 16.5 %while.10 = (s32[]{:T(128)}, f32[384,128]{1,0:T(8,128)S(1)}, f32[384,128]{1,0:T(8,128)S(1)}, bf16[512,512]{1,0:T(8,128)(2,1)}, bf16[384,128]{1,0:T(8,128)(2,1)},...) while((s32[]{:T(128)}, f32[384,128]{1,0:T(8,128)S(1)}, ...), condition=%wide.region_8.9_spmd.clone, body=%wide.region_7.8_spmd.clone.sunk | while | flops 405258240 | bytes 8872134 | solution.py:153
  109.2 1.1 constant_dynamic-slice_fusion.7
  110.3 0.1 copy.71
  110.4 2.6 %exponential_divide_fusion.2 = f32[256,4,384]{2,0,1:T(8,128)} fusion(bf16[256,4,128]{0,2,1:T(8,128)(2,1)S(1)} %bitcast.95, f32[256,4]{0,1:T(4,128)S(1)} %get-tuple-element.326, bf16[384,128]{1,0:T(8,128)(2,1)} %get-tuple-element.359), kind=kOutput, calls=%fused_computation.1.clone.1 | convolution fusion | flops 101449728 | bytes 1937408 | tf_op jit(solution)/shard_map/while/body/eval_jaxpr/ihd,jd->ihj/dot_general | solution.py:132
  113.0 0.1 copy.72
  113.1 2.5 %fusion.92 = f32[384,128]{1,0:T(8,128)S(1)} fusion(bf16[256,4,128]{0,2,1:T(8,128)(2,1)S(1)} %bitcast.96, f32[256,4,384]{2,0,1:T(8,128)} %exponential_divide_fusion.2, bf16[256,4,128]{0,2,1:T(8,128)(2,1)S(1)} %bitcast.93, f32[256,4]{0,1:T(4,128)S(1)} %get-tuple-element.328, f32[384,128]{1,0:T(8,128)S(1)} %get-tuple-element.343, ...), kind=kOutput, calls=%fused_computation.6.clone.1 | convolution fusion | flops 202653696 | bytes 2592769 | tf_op jit(solution)/shard_map/while/body/eval_jaxpr/ihj,ihd->jd/dot_general | solution.py:142
  115.6 1.8 fusion.93
  117.5 1.1 constant_dynamic-slice_fusion.7
  118.5 0.1 copy.71
  118.7 2.6 %exponential_divide_fusion.2 = f32[256,4,384]{2,0,1:T(8,128)} fusion(bf16[256,4,128]{0,2,1:T(8,128)(2,1)S(1)} %bitcast.95, f32[256,4]{0,1:T(4,128)S(1)} %get-tuple-element.326, bf16[384,128]{1,0:T(8,128)(2,1)} %get-tuple-element.359), kind=kOutput, calls=%fused_computation.1.clone.1 | convolution fusion | flops 101449728 | bytes 1937408 | tf_op jit(solution)/shard_map/while/body/eval_jaxpr/ihd,jd->ihj/dot_general | solution.py:132
  121.3 0.1 copy.72
  121.4 2.5 %fusion.92 = f32[384,128]{1,0:T(8,128)S(1)} fusion(bf16[256,4,128]{0,2,1:T(8,128)(2,1)S(1)} %bitcast.96, f32[256,4,384]{2,0,1:T(8,128)} %exponential_divide_fusion.2, bf16[256,4,128]{0,2,1:T(8,128)(2,1)S(1)} %bitcast.93, f32[256,4]{0,1:T(4,128)S(1)} %get-tuple-element.328, f32[384,128]{1,0:T(8,128)S(1)} %get-tuple-element.343, ...), kind=kOutput, calls=%fused_computation.6.clone.1 | convolution fusion | flops 202653696 | bytes 2592769 | tf_op jit(solution)/shard_map/while/body/eval_jaxpr/ihj,ihd->jd/dot_general | solution.py:142
  123.9 1.8 fusion.93
  125.7 0.6 convert_element_type.105
  126.4 0.0 reduce-scatter.6.cloned.1.call-update
  126.4 0.0 reduce-scatter.8.cloned.1.call-start
  126.5 3.2 %fusion.17 = bf16[128,4,128]{0,2,1:T(8,128)(2,1)S(1)} fusion(f32[128,4,128]{0,2,1:T(8,128)} %convolution_multiply_fusion.2, f32[128,4,1536]{2,0,1:T(8,128)} %get-tuple-element.261, bf16[128,4,128]{0,2,1:T(8,128)(2,1)S(1)} %bitcast.98, bf16[1536,128]{1,0:T(8,128)(2,1)} %copy-done.3, bf16[1536,128]{1,0:T(8,128)(2,1)} %copy-done.2, ...), kind=kOutput, calls=%fused_computation.32 | convolution fusion | flops 404488192 | bytes 4458496 | tf_op jit(solution)/shard_map/while/body/eval_jaxpr/ihj,jd->ihd/dot_general | solution.py:89
  129.7 0.6 convert_element_type.106
  130.3 0.0 reduce-scatter.8.cloned.1.call-update
  130.3 0.0 reduce-scatter.4.cloned.1.call-start
  130.4 1.6 convolution_convert_fusion
  132.0 0.0 reduce-scatter.4.cloned.1.call-update
  132.0 1.0 fusion.48
  133.0 9.9 %all_gather.31 = bf16[512,512]{0,1:T(8,128)(2,1)S(1)} all-gather(bf16[128,512]{0,1:T(8,128)(2,1)S(1)} %bitcast.99), channel_id=1, replica_groups=mesh['sp'=4,'tp'=8] {'sp'}, dimensions={0}, use_global_device_ids=true | all-gather | bytes 655360 | tf_op jit(solution)/shard_map/all_gather | solution.py:180
  143.0 2.1 copy.46
  145.1 2.3 convolution_convert_fusion.1
  147.3 9.8 %reduce-scatter.6.cloned.1.call-done = bf16[48,128]{1,0:T(8,128)(2,1)} async-done(((bf16[384,128]{1,0:T(8,128)(2,1)}), bf16[48,128]{1,0:T(8,128)(2,1)}) %reduce-scatter.6.cloned.1.call-update) | async-done | bytes 12304 | tf_op jit(solution)/shard_map/reduce_scatter | solution.py:157
  157.2 1.3 fusion.56
  158.5 29.7 %reduce-scatter.8.cloned.1.call-done = bf16[48,128]{1,0:T(8,128)(2,1)} async-done(((bf16[384,128]{1,0:T(8,128)(2,1)}), bf16[48,128]{1,0:T(8,128)(2,1)}) %reduce-scatter.8.cloned.1.call-update) | async-done | bytes 12304 | tf_op jit(solution)/shard_map/reduce_scatter | solution.py:160
  188.2 1.3 fusion.31
  189.6 1.7 fusion.34
  191.3 28.5 %reduce-scatter.4.cloned.1.call-done = bf16[16,2048]{1,0:T(8,128)(2,1)} async-done(((bf16[128,2048]{1,0:T(8,128)(2,1)}), bf16[16,2048]{1,0:T(8,128)(2,1)}) %reduce-scatter.4.cloned.1.call-update) | async-done | bytes 65552 | tf_op jit(solution)/shard_map/reduce_scatter | solution.py:170
  219.8 1.1 fusion.44
  220.9 1.6 fusion.47
  (45 shorter events, 0.2 us)
Async XLA Ops:
  7.2 37.8 %copy-start = (bf16[2048,512]{1,0:T(8,128)(2,1)S(1)}, bf16[2048,512]{1,0:T(8,128)(2,1)}, u32[]{:S(2)}) copy-start(bf16[2048,512]{1,0:T(8,128)(2,1)} %param.16) | copy-start | bytes 6291460
  7.2 5.8 %copy-start.7 = (bf16[128,2048]{1,0:T(8,128)(2,1)S(1)}, bf16[128,2048]{1,0:T(8,128)(2,1)}, u32[]{:S(2)}) copy-start(bf16[128,2048]{1,0:T(8,128)(2,1)} %param.13) | copy-start | bytes 1572868
  9.9 9.5 %copy-start.6 = (bf16[2048,128]{1,0:T(8,128)(2,1)S(1)}, bf16[2048,128]{1,0:T(8,128)(2,1)}, u32[]{:S(2)}) copy-start(bf16[2048,128]{1,0:T(8,128)(2,1)} %param.17) | copy-start | bytes 1572868
  9.9 9.5 %copy-start.13 = (f32[2048]{0:T(1024)S(1)}, f32[2048]{0:T(1024)}, u32[]{:S(2)}) copy-start(f32[2048]{0:T(1024)} %param.15) | copy-start | bytes 24580
  10.0 62.5 %collective-permute-start = (bf16[128,512]{1,0:T(8,128)(2,1)S(1)}, bf16[128,512]{1,0:T(8,128)(2,1)}, u32[]{:S(2)}, u32[]{:S(2)}) collective-permute-start(bf16[128,512]{1,0:T(8,128)(2,1)S(1)} %convolution_convert_fusion.2), channel_id=1, source_target_pairs={{0,8},{8,16},{16,24},{24,0},{1,9},{9,17},{17,25},{25,1},{2,10},{10... | collective-permute-start | bytes 393224 | tf_op jit(solution)/shard_map/ppermute | solution.py:113
  14.0 30.7 %copy-start.8 = (bf16[128,2048]{1,0:T(8,128)(2,1)S(1)}, bf16[128,2048]{1,0:T(8,128)(2,1)}, u32[]{:S(2)}) copy-start(bf16[128,2048]{1,0:T(8,128)(2,1)} %param.11) | copy-start | bytes 1572868
  14.0 30.9 %copy-start.14 = (f32[2048]{0:T(1024)S(1)}, f32[2048]{0:T(1024)}, u32[]{:S(2)}) copy-start(f32[2048]{0:T(1024)} %param.14) | copy-start | bytes 24580
  14.0 128.9 %all-to-all-start = ((bf16[128,4,512]{0,2,1:T(8,128)(2,1)}), bf16[128,4,512]{0,2,1:T(8,128)(2,1)}, u32[]{:S(2)}, u32[]{:S(2)}) async-start(bf16[128,4,512]{0,2,1:T(8,128)(2,1)} %bitcast.7), calls=%async_computation.3 | async-start | bytes 1048576 | tf_op jit(solution)/shard_map/all_to_all | solution.py:49
  18.3 138.9 %reduce-scatter.6.cloned.1.call-start = ((), (), s32[]{:S(2)}) async-start(), calls=%async_computation.5 | async-start | bytes 110592 | tf_op jit(solution)/shard_map/reduce_scatter | solution.py:157
  34.8 10.1 %copy-start.12 = (bf16[384,128]{1,0:T(8,128)(2,1)}, bf16[384,128]{1,0:T(8,128)(2,1)S(1)}, u32[]{:S(2)}) copy-start(bf16[384,128]{1,0:T(8,128)(2,1)S(1)} %all_gather.24) | copy-start | bytes 294916
  44.7 33.9 %copy-start.2 = (bf16[1536,128]{1,0:T(8,128)(2,1)}, bf16[1536,128]{1,0:T(8,128)(2,1)S(1)}, u32[]{:S(2)}) copy-start(bf16[1536,128]{1,0:T(8,128)(2,1)S(1)} %all_gather.25) | copy-start | bytes 1179652
  45.4 2.3 %copy-start.10 = (bf16[128,512]{1,0:T(8,128)(2,1)}, bf16[128,512]{1,0:T(8,128)(2,1)S(1)}, u32[]{:S(2)}) copy-start(bf16[128,512]{1,0:T(8,128)(2,1)S(1)} %convolution_convert_fusion.3) | copy-start | bytes 393220
  45.5 2.3 copy-start.4
  72.4 4.0 %copy-start.3 = (bf16[1536,128]{1,0:T(8,128)(2,1)}, bf16[1536,128]{1,0:T(8,128)(2,1)S(1)}, u32[]{:S(2)}) copy-start(bf16[1536,128]{1,0:T(8,128)(2,1)S(1)} %all_gather.27) | copy-start | bytes 1179652
  72.5 6.1 %collective-permute-start.1 = (bf16[128,512]{1,0:T(8,128)(2,1)}, bf16[128,512]{1,0:T(8,128)(2,1)S(1)}, u32[]{:S(2)}, u32[]{:S(2)}) collective-permute-start(bf16[128,512]{1,0:T(8,128)(2,1)} %collective-permute-done), channel_id=1, source_target_pairs={{0,8},{8,16},{16,24},{24,0},{1,9},{9,17},{17,25},{25,1},{2,10},{10... | collective-permute-start | bytes 393224 | tf_op jit(solution)/shard_map/ppermute | solution.py:113
  73.1 5.5 %copy-start.1 = (f32[128,4,1536]{2,0,1:T(8,128)S(1)}, f32[128,4,1536]{2,0,1:T(8,128)}, u32[]{:S(2)}) copy-start(f32[128,4,1536]{2,0,1:T(8,128)} %get-tuple-element.261) | copy-start | bytes 9437188
  78.6 27.8 %collective-permute-start.2 = (bf16[128,512]{1,0:T(8,128)(2,1)S(1)}, bf16[128,512]{1,0:T(8,128)(2,1)S(1)}, u32[]{:S(2)}, u32[]{:S(2)}) collective-permute-start(bf16[128,512]{1,0:T(8,128)(2,1)S(1)} %collective-permute-done.1), channel_id=1, source_target_pairs={{0,8},{8,16},{16,24},{24,0},{1,9},{9,17},{17,25},{25,1},{2,10},{10... | collective-permute-start | bytes 393224 | tf_op jit(solution)/shard_map/ppermute | solution.py:113
  78.6 18.0 %copy-start.11 = (bf16[128,512]{1,0:T(8,128)(2,1)S(1)}, bf16[128,512]{1,0:T(8,128)(2,1)}, u32[]{:S(2)}) copy-start(bf16[128,512]{1,0:T(8,128)(2,1)} %copy-done.10) | copy-start | bytes 393220
  126.4 61.8 %reduce-scatter.8.cloned.1.call-start = ((), (), s32[]{:S(2)}) async-start(), calls=%async_computation.6 | async-start | bytes 110592 | tf_op jit(solution)/shard_map/reduce_scatter | solution.py:160
  130.3 89.5 %reduce-scatter.4.cloned.1.call-start = ((), (), s32[]{:S(2)}) async-start(), calls=%async_computation.4 | async-start | bytes 589824 | tf_op jit(solution)/shard_map/reduce_scatter | solution.py:170
  130.4 2.6 %copy-start.9 = (bf16[128,4,128]{0,2,1:T(8,128)(2,1)S(1)}, bf16[128,4,128]{0,2,1:T(8,128)(2,1)}, u32[]{:S(2)}) copy-start(bf16[128,4,128]{0,2,1:T(8,128)(2,1)} %get-tuple-element.263) | copy-start | bytes 393220
  143.0 45.2 %copy-start.5 = (bf16[2048,128]{1,0:T(8,128)(2,1)S(1)}, bf16[2048,128]{1,0:T(8,128)(2,1)}, u32[]{:S(2)}) copy-start(bf16[2048,128]{1,0:T(8,128)(2,1)} %param.18) | copy-start | bytes 1572868
Sparse Core Ops, SparseCore 0:
  126.5 30.6 reduce-scatter.5
  159.4 28.7 reduce-scatter.7
  190.5 29.2 reduce-scatter.3
